TPU v7x, 128 devices: a whole 4x4x4 slice. The times are simulated.
128 devices in a mesh: sp: 16 (over z, y), dp: 8 (over x, core).
Axes of the slice: x: 4, y: 4, z: 4, core: 2. Of those that a mesh axis runs over, the one named last changes fastest.
Arguments:
- u_pre: bfloat16 [8, 16384, 2048], P('dp', 'sp'), may hold values from -6 to 6
- v_pre: bfloat16 [8, 16384, 2048], P('dp', 'sp'), may hold values from -6 to 6
- d_out: bfloat16 [8, 16384, 2048], P('dp', 'sp'), may hold values from -6 to 6
- w_mix: bfloat16 [16, 128, 128], replicated, may hold values from -0.5 to 0.5
- mix_bias: float32 [16, 128], replicated, may hold values from 0.1 to 1.9
- norm_gain: float32 [16, 128], replicated, may hold values from 0.1 to 1.9
- norm_shift: float32 [16, 128], replicated, may hold values from -3 to 3
- w_out: bfloat16 [2048, 2048], P('dp'), may hold values from -0.125 to 0.125
Outputs:
- grad_u: bfloat16 [8, 16384, 2048], P('dp', 'sp')
- grad_v: bfloat16 [8, 16384, 2048], P('dp', 'sp')
- grad_w_out: float32 [2048, 2048], P('dp')
- grad_w_mix: float32 [16, 128, 128], replicated
- grad_mix_bias: float32 [16, 128], replicated
- grad_gain: float32 [16, 128], replicated
- grad_shift: float32 [16, 128], replicated
All inputs are finite; a program needn't handle non-finite values.
Results may differ from a plain program's by a relative error of at most 0.012.
Values may be sent and summed in bfloat16 or wider, within the bound.
A program may use at most 192 MiB of HBM per device.

v0:
```python
import jax
import jax.numpy as jnp
from jax import lax
from jax.sharding import PartitionSpec as P

EPS = 1e-05


def together(arrays, axis):
    ends = [0]
    for a in arrays:
        ends.append(ends[-1] + a.size)
    total = lax.psum(jnp.concatenate([a.ravel() for a in arrays]), axis)
    return tuple((total[b:e].reshape(a.shape) for a, b, e in zip(arrays, ends, ends[1:])))


def mechanism(grad_s, u_pre, v_pre, w_mix, mix_bias, gain, shift):
    items, length, width = grad_s.shape
    groups, span = (w_mix.shape[0], w_mix.shape[1])
    chans = width // groups
    shape = (items, length // span, span, groups, chans)
    u_val = u_pre.astype(jnp.float32).reshape(shape)
    v_val = v_pre.astype(jnp.float32).reshape(shape)
    cotan = grad_s.astype(jnp.float32).reshape(shape)
    upper, u_back = jax.vjp(jax.nn.gelu, u_val)
    gated, v_back = jax.vjp(jax.nn.gelu, v_val)
    centre = gated - jnp.mean(gated, axis=-1, keepdims=True)
    inverse = lax.rsqrt(jnp.mean(centre * centre, axis=-1, keepdims=True) + EPS)
    scaled = centre * inverse
    normed = (scaled * gain + shift).astype(jnp.bfloat16)
    lower = jnp.tril(jnp.ones((span, span), dtype=bool))
    w_low = jnp.where(lower[None], w_mix, jnp.zeros_like(w_mix))
    mixed = jnp.einsum("gts,insgc->intgc", w_low, normed, preferred_element_type=jnp.float32)
    mixed = mixed + jnp.transpose(mix_bias)[:, :, None]
    gated_out = (upper * mixed).astype(jnp.bfloat16)
    d_mixed = cotan * upper
    d_mixed_b = d_mixed.astype(jnp.bfloat16)
    grad_u = u_back(cotan * mixed)[0].astype(jnp.bfloat16).reshape(items, length, width)
    grad_bias = jnp.transpose(jnp.sum(d_mixed, axis=(0, 1, 4)))
    grad_w = jnp.einsum("intgc,insgc->gts", d_mixed_b, normed, preferred_element_type=jnp.float32)
    grad_w = jnp.where(lower[None], grad_w, jnp.zeros_like(grad_w))
    d_normed = jnp.einsum("gts,intgc->insgc", w_low, d_mixed_b, preferred_element_type=jnp.float32)
    grad_gain = jnp.sum(d_normed * scaled, axis=(0, 1, 2))
    grad_shift = jnp.sum(d_normed, axis=(0, 1, 2))
    d_scaled = d_normed * gain
    d_gated = inverse * (
        d_scaled
        - jnp.mean(d_scaled, axis=-1, keepdims=True)
        - scaled * jnp.mean(d_scaled * scaled, axis=-1, keepdims=True)
    )
    grad_v = v_back(d_gated)[0].astype(jnp.bfloat16).reshape(items, length, width)
    return (
        grad_u,
        grad_v,
        gated_out.reshape(items, length, width),
        grad_w,
        grad_bias,
        grad_gain,
        grad_shift,
    )


def on_device(u_pre, v_pre, d_out, w_mix, mix_bias, norm_gain, norm_shift, w_out):
    grad_s = lax.dot_general(
        d_out,
        lax.all_gather(w_out, "dp", axis=0, tiled=True),
        (((2,), (1,)), ((), ())),
        preferred_element_type=jnp.float32,
    ).astype(jnp.bfloat16)
    grad_u, grad_v, gated_out, grad_w, grad_bias, grad_gain, grad_shift = mechanism(
        grad_s, u_pre, v_pre, w_mix, mix_bias, norm_gain, norm_shift
    )
    grad_w, grad_bias, grad_gain, grad_shift = together(
        (grad_w, grad_bias, grad_gain, grad_shift), ("sp", "dp")
    )
    width = gated_out.shape[2]
    flat_d = d_out.reshape(-1, d_out.shape[2])
    flat_s = gated_out.reshape(-1, width)
    partial_rows = lax.psum_scatter(
        lax.dot_general(
            flat_s, flat_d, (((0,), (0,)), ((), ())), preferred_element_type=jnp.float32
        ),
        "dp",
        scatter_dimension=0,
        tiled=True,
    )
    grad_w_out = lax.psum(partial_rows, "sp")
    return (grad_u, grad_v, grad_w_out, grad_w, grad_bias, grad_gain, grad_shift)


def solution(mesh):
    return jax.shard_map(
        on_device,
        mesh=mesh,
        in_specs=(
            P("dp", "sp", None),
            P("dp", "sp", None),
            P("dp", "sp", None),
            P(),
            P(),
            P(),
            P(),
            P("dp", None),
        ),
        out_specs=(P("dp", "sp", None), P("dp", "sp", None), P("dp", None), P(), P(), P(), P()),
        check_vma=False,
    )
```

profile of v0, /device:TPU:0, one launch (start us, length us, event | category | flops | bytes accessed | tf_op | source)
XLA Modules:
  0.0 474.1 jit_solution(16673040196392679940)
XLA Ops:
  7.2 0.7 all-gather.2.cloned.1.call-update
  7.9 3.2 convert_bitcast_fusion
  11.2 5.2 %copy.67 = f32[128,8,16,128]{3,2,1,0:T(8,128)} copy(f32[128,8,16,128]{3,1,2,0:T(8,128)S(1)} %convert_bitcast_fusion) | data formatting | bytes 16777216
  16.4 9.1 %copy.45 = f32[1,8,128,16,128]{2,4,1,3,0:T(8,128)} copy(f32[1,8,128,16,128]{4,3,0,2,1:T(8,128)} %bitcast.100) | data formatting | bytes 16777216 | tf_op jit(solution)/shard_map/reshape | solution.py:22
  25.5 3.2 convert_bitcast_fusion.1
  28.8 5.2 %copy.65 = f32[128,8,16,128]{3,2,1,0:T(8,128)} copy(f32[128,8,16,128]{3,1,2,0:T(8,128)S(1)} %convert_bitcast_fusion.1) | data formatting | bytes 16777216
  34.0 8.7 %copy.39 = f32[1,8,128,16,128]{2,4,1,3,0:T(8,128)} copy(f32[1,8,128,16,128]{4,3,0,2,1:T(8,128)} %bitcast.104) | data formatting | bytes 16777216 | tf_op jit(solution)/shard_map/reshape | solution.py:23
  42.8 5.9 %fusion.54 = f32[8,128,16]{1,0,2:T(8,128)S(1)} fusion(f32[1,8,128,16,128]{2,4,1,3,0:T(8,128)} %copy.39), kind=kLoop, calls=%fused_computation.83 | loop fusion | flops 18857984 | bytes 8454144 | tf_op jit(solution)/shard_map/reduce_sum | solution.py:27
  48.9 3.7 multiply_reduce_fusion.2
  52.7 6.5 %fusion.35 = bf16[8,128,16,128]{3,1,0,2:T(8,128)(2,1)} fusion(f32[8,128,16,128]{3,2,1,0:T(8,128)S(1)} %bitcast.105, f32[16,128]{1,0:T(8,128)S(1)} %copy-done.4, f32[16,128]{1,0:T(8,128)S(1)} %copy-done.3, f32[8,128,16]{1,0,2:T(8,128)S(1)} %add_rsqrt_fusion, f32[8,128,16]{1,0,2:T(8,128)S(1)} %broadcast_multiply_fusion.2), kind=kLoop, calls=%fused_computation.52 | loop fusion | flops 27262976 | bytes 12730368 | tf_op jit(solution)/shard_map/convert_element_type | solution.py:30
  59.1 2.7 all-gather.2.cloned.1.call-done
  61.8 13.1 %convert_bitcast_fusion.2 = f32[128,8,16,128]{3,1,2,0:T(8,128)S(1)} fusion(bf16[2048,2048]{1,0:T(8,128)(2,1)} %all-gather.2.cloned.1.call-done, bf16[1,1024,2048]{2,1,0:T(8,128)(2,1)} %param.10), kind=kOutput, calls=%fused_computation.51 | convolution fusion | flops 8594128896 | bytes 20971520 | tf_op jit(solution)/shard_map/dot_general | solution.py:64
  74.9 5.2 %copy.64 = f32[128,8,16,128]{3,2,1,0:T(8,128)} copy(f32[128,8,16,128]{3,1,2,0:T(8,128)S(1)} %convert_bitcast_fusion.2) | data formatting | bytes 16777216
  80.1 8.8 %copy.41 = f32[1,8,128,16,128]{2,4,1,3,0:T(8,128)} copy(f32[1,8,128,16,128]{4,3,2,1,0:T(8,128)} %bitcast.102) | data formatting | bytes 16777216 | tf_op jit(solution)/shard_map/reshape | solution.py:24
  88.9 14.8 %multiply_convert_fusion = (bf16[1,8,128,16,128]{2,4,1,3,0:T(8,128)(2,1)}, bf16[1,8,128,16,128]{2,4,1,3,0:T(8,128)(2,1)}, f32[128,16]{0,1:T(8,128)S(1)}) fusion(f32[128,16]{0,1:T(8,128)S(1)} %bitcast.112, f32[1,8,128,16,128]{2,4,1,3,0:T(8,128)} %copy.45, f32[1,8,128,16,128]{2,4,1,3,0:T(8,128)} %copy.41, bf16[8,128,16,128]{3,1,0,2:T(8,128)(2,1)} %fusion.35, ...), kind=kOutput, calls=%fused_computation.46 | convolution fusion | flops 593754112 | bytes 29917184 | tf_op jit(solution)/shard_map/gts,insgc->intgc/dot_general | solution.py:33
  103.7 6.8 %copy.58 = bf16[1,8,128,16,128]{4,3,2,1,0:T(8,128)(2,1)} copy(bf16[1,8,128,16,128]{2,4,1,3,0:T(8,128)(2,1)} %get-tuple-element.11) | data formatting | bytes 8388608 | tf_op jit(solution)/shard_map/convert_element_type | solution.py:35
  110.5 15.4 %fusion.37 = f32[2048,2048]{1,0:T(8,128)} fusion(bf16[128,8,16,128]{3,2,1,0:T(8,128)(2,1)} %bitcast.107, bf16[1,1024,2048]{2,1,0:T(8,128)(2,1)} %param.10), kind=kOutput, calls=%fused_computation.57 | convolution fusion | flops 8589934592 | bytes 25165824 | tf_op jit(solution)/shard_map/dot_general | solution.py:80
  125.9 10.2 %fusion.33 = bf16[8,128,16,128]{3,1,0,2:T(8,128)(2,1)S(1)} fusion(f32[8,128,16,128]{3,2,1,0:T(8,128)} %bitcast.103, f32[8,128,16,128]{3,2,1,0:T(8,128)} %bitcast.101), kind=kLoop, calls=%fused_computation.39 | loop fusion | flops 20971520 | bytes 20971520 | tf_op jit(solution)/shard_map/convert_element_type | solution.py:37
  136.2 1.3 fusion.45
  137.4 10.3 %fusion.34 = (f32[16,128]{1,0:T(8,128)S(1)}, f32[8,128,16]{1,0,2:T(8,128)S(1)}, f32[8,128,16]{1,0,2:T(8,128)S(1)}, f32[16,128]{1,0:T(8,128)S(1)}, f32[16,8,128,128]{3,2,1,0:T(8,128)}) fusion(f32[8,128,16]{1,0,2:T(8,128)S(1)} %add_rsqrt_fusion, f32[8,128,16]{1,0,2:T(8,128)S(1)} %broadcast_multiply_fusion.2, f32[1,8,128,16,128]{2,4,1,3,0:T(8,128)} %copy.39, ...), kind=kOutput, calls=%fused_computation.44 | convolution fusion | flops 572747776 | bytes 21798912 | tf_op jit(solution)/shard_map/gts,intgc->insgc/dot_general | solution.py:42
  147.7 1.0 pad_maximum_fusion
  148.9 7.0 %copy.47 = bf16[1,8,128,16,128]{4,3,2,1,0:T(8,128)(2,1)} copy(bf16[1,8,128,16,128]{2,4,1,3,0:T(8,128)(2,1)} %get-tuple-element.12) | data formatting | bytes 8388608 | tf_op jit(solution)/shard_map/convert_element_type | solution.py:38
  155.8 7.3 %reshape.497 = bf16[1,1024,2048]{2,1,0:T(8,128)(2,1)} reshape(bf16[1,8,128,16,128]{4,3,2,1,0:T(8,128)(2,1)} %copy.47) | data formatting | bytes 8388608 | tf_op jit(solution)/shard_map/reshape | solution.py:38
  163.2 54.8 %reduce-scatter.2.cloned.1.call-done = f32[256,2048]{1,0:T(8,128)} async-done(((f32[2048,2048]{1,0:T(8,128)}), f32[256,2048]{1,0:T(8,128)}) %reduce-scatter.2.cloned.1.call-update) | async-done | bytes 2097168 | tf_op jit(solution)/shard_map/reduce_scatter | solution.py:79
  218.0 12.0 %fusion.6 = bf16[1,8,128,16,128]{2,4,1,3,0:T(8,128)(2,1)} fusion(f32[1,8,128,16,128]{2,4,1,3,0:T(8,128)} %copy.39, f32[16,8,128,128]{3,2,1,0:T(8,128)} %get-tuple-element.17, f32[8,128,16]{1,0,2:T(8,128)S(1)} %get-tuple-element.18, f32[8,128,16]{1,0,2:T(8,128)S(1)} %get-tuple-element.19, f32[16,128]{1,0:T(8,128)S(1)} %copy-done.3, ...), kind=kLoop, calls=%fused_computation.12 | loop fusion | flops 58720256 | bytes 21241856 | tf_op jit(solution)/shard_map/convert_element_type | solution.py:51
  230.0 6.7 %copy.56 = bf16[1,8,128,16,128]{4,3,2,1,0:T(8,128)(2,1)} copy(bf16[1,8,128,16,128]{2,4,1,3,0:T(8,128)(2,1)} %fusion.6) | data formatting | bytes 8388608 | tf_op jit(solution)/shard_map/convert_element_type | solution.py:51
  236.8 7.3 %reshape.500 = bf16[1,1024,2048]{2,1,0:T(8,128)(2,1)} reshape(bf16[1,8,128,16,128]{4,3,2,1,0:T(8,128)(2,1)} %copy.56) | data formatting | bytes 8388608 | tf_op jit(solution)/shard_map/reshape | solution.py:51
  244.1 127.2 %all-reduce.5.cloned.1.call-done = f32[268288]{0:T(1024)} async-done(((f32[268288]{0:T(1024)}), f32[268288]{0:T(1024)}) %all-reduce.5.cloned.1.call-update) | async-done | bytes 1073168 | tf_op jit(solution)/shard_map/psum | solution.py:13
  371.2 2.3 slice.49
  373.5 1.3 slice_bitcast_fusion
  374.8 89.4 %all-reduce.3.cloned.1.call-done = f32[256,2048]{1,0:T(8,128)} async-done(((f32[256,2048]{1,0:T(8,128)}), f32[256,2048]{1,0:T(8,128)}) %all-reduce.3.cloned.1.call-update) | async-done | bytes 2097168 | tf_op jit(solution)/shard_map/psum | solution.py:87
  464.2 3.1 copy.82
  (25 shorter events, 0.5 us)
Async XLA Ops:
  7.2 54.7 %all-gather.2.cloned.1.call-start = ((), (), s32[]{:S(2)}) async-start(), calls=%async_computation.1 | async-start | bytes 9437184 | tf_op jit(solution)/shard_map/all_gather | solution.py:66
  7.9 210.1 %reduce-scatter.2.cloned.1.call-start = ((), (), s32[]{:S(2)}) async-start(), calls=%async_computation.2 | async-start | bytes 18874368 | tf_op jit(solution)/shard_map/reduce_scatter | solution.py:79
  42.7 6.2 %copy-start = (f32[1,8,128,16,128]{2,4,1,3,0:T(8,128)S(1)}, f32[1,8,128,16,128]{2,4,1,3,0:T(8,128)}, u32[]{:S(2)}) copy-start(f32[1,8,128,16,128]{2,4,1,3,0:T(8,128)} %copy.39) | copy-start | bytes 25165828
  42.7 9.9 %copy-start.1 = (f32[128,8,16,128]{3,2,1,0:T(8,128)S(1)}, f32[128,8,16,128]{3,2,1,0:T(8,128)}, u32[]{:S(2)}) copy-start(f32[128,8,16,128]{3,2,1,0:T(8,128)} %copy.65) | copy-start | bytes 25165828
  42.7 9.9 %copy-start.3 = (f32[16,128]{1,0:T(8,128)S(1)}, f32[16,128]{1,0:T(8,128)}, u32[]{:S(2)}) copy-start(f32[16,128]{1,0:T(8,128)} %param.13) | copy-start | bytes 24580
  42.7 9.9 %copy-start.4 = (f32[16,128]{1,0:T(8,128)S(1)}, f32[16,128]{1,0:T(8,128)}, u32[]{:S(2)}) copy-start(f32[16,128]{1,0:T(8,128)} %param.14) | copy-start | bytes 24580
  80.1 8.8 %copy-start.5 = (bf16[16,128,128]{2,1,0:T(8,128)(2,1)S(1)}, bf16[16,128,128]{2,1,0:T(8,128)(2,1)}, u32[]{:S(2)}) copy-start(bf16[16,128,128]{2,1,0:T(8,128)(2,1)} %param.11) | copy-start | bytes 1572868
  80.1 8.8 %copy-start.6 = (f32[16,128]{1,0:T(8,128)S(1)}, f32[16,128]{1,0:T(8,128)}, u32[]{:S(2)}) copy-start(f32[16,128]{1,0:T(8,128)} %param.12) | copy-start | bytes 24580
  125.9 245.4 %all-reduce.5.cloned.1.call-start = ((), (), s32[]{:S(2)}) async-start(), calls=%async_computation.4 | async-start | bytes 2146304 | tf_op jit(solution)/shard_map/psum | solution.py:13
  125.9 10.2 %copy-start.2 = (bf16[8,128,16,128]{3,1,0,2:T(8,128)(2,1)S(1)}, bf16[8,128,16,128]{3,1,0,2:T(8,128)(2,1)}, u32[]{:S(2)}) copy-start(bf16[8,128,16,128]{3,1,0,2:T(8,128)(2,1)} %fusion.35) | copy-start | bytes 12582916
  148.8 315.4 %all-reduce.3.cloned.1.call-start = ((), (), s32[]{:S(2)}) async-start(), calls=%async_computation.3 | async-start | bytes 4194304 | tf_op jit(solution)/shard_map/psum | solution.py:87
Sparse Core Ops, SparseCore 0:
  9.7 52.0 all-gather.1
  126.0 91.9 reduce-scatter.1
  223.3 147.8 all-reduce.4
  374.4 89.7 all-reduce.2
where the time goes:
time: 478 us; the launch traced here: 474 us
  waiting for transfers between devices  275 us (58%)
  local copies, waits for them, and re-layouts  84.4 us (18%)
  matrix products  54.8 us (11%)
  other arithmetic  45.8 us (10%)
  between operations  14.1 us (3%)
    psum x1, waiting for transfers between devices, together(): total = lax.psum(jnp.concatenate([a.ravel() for a in arrays]), axis)  127 us
    psum x1, waiting for transfers between devices, on_device(): grad_w_out = lax.psum(partial_rows, 'sp')  89.4 us
    reduce_scatter x1, waiting for transfers between devices, on_device(): lax.psum_scatter(lax.dot_general(flat_s, flat_d, (((0,), (0,)), ((), ()))...  54.8 us
    unnamed x18, local copies, waits for them, and re-layouts  19 us
    dot_general x1, matrix products, on_device(): lax.dot_general(flat_s, flat_d, (((0,), (0,)), ((), ())), preferred_eleme...  15.4 us
    dot_general x1, matrix products, mechanism(): jnp.einsum('gts,insgc->intgc', w_low, normed, preferred_element_type=jnp....  14.8 us
    dot_general x1, matrix products, on_device(): lax.dot_general(d_out, lax.all_gather(w_out, 'dp', axis=0, tiled=True), (...  13.1 us
    convert_element_type x1, other arithmetic, mechanism(): v_back(d_gated)[0].astype(jnp.bfloat16).reshape(items, length, width)  12 us
  transfers between devices with their start and end apart: 4, of which 4 were waited for; matrix products, arithmetic and copies ran while one was open for 25% of the time, Pallas kernels for 0%

commit v1 on v0

--- a/solution.py
+++ b/solution.py
@@ -84,7 +84,7 @@
         scatter_dimension=0,
         tiled=True,
     )
-    grad_w_out = lax.psum(partial_rows, "sp")
+    grad_w_out = jnp.sum(lax.all_gather(partial_rows, "sp"), axis=0)
     return (grad_u, grad_v, grad_w_out, grad_w, grad_bias, grad_gain, grad_shift)
 
 

time: 478 us -> 594 us (1.24)
  waiting for transfers between devices: 275 us -> 379 us
  other arithmetic: 45.8 us -> 59.3 us
    all_gather x0 -> x1, waiting for transfers between devices: none -> 194 us  [on_device(): grad_w_out = jnp.sum(lax.all_gather(partial_rows, 'sp'), axis=0)]
    psum x1 -> x0, waiting for transfers between devices: 89.4 us -> none  [on_device(): grad_w_out = lax.psum(partial_rows, 'sp')]
    psum x1, waiting for transfers between devices: 127 us -> 113 us  [together(): total = lax.psum(jnp.concatenate([a.ravel() for a in arrays]), axis)]
    reduce_scatter x1, waiting for transfers between devices: 54.8 us -> 69.1 us  [on_device(): lax.psum_scatter(lax.dot_general(flat_s, flat_d, (((0,), (0,)), ((), ()))...]
    reduce_sum x0 -> x1, other arithmetic: none -> 13.1 us  [on_device(): grad_w_out = jnp.sum(lax.all_gather(partial_rows, 'sp'), axis=0)]
    unnamed x18 -> x17, local copies, waits for them, and re-layouts: 19 us -> 15.7 us
  transfers between devices with their start and end apart: 4 -> 4, of which waited for: 4 -> 4; matrix products, arithmetic and copies ran while one was open for 25% -> 20% of each run, Pallas kernels for 0% -> 0%
where the time goes in v1:
time: 594 us; the launch traced here: 589 us
  waiting for transfers between devices  379 us (64%)
  local copies, waits for them, and re-layouts  81 us (14%)
  other arithmetic  59.3 us (10%)
  matrix products  54.9 us (9%)
  between operations  14.1 us (2%)
    all_gather x1, waiting for transfers between devices, on_device(): grad_w_out = jnp.sum(lax.all_gather(partial_rows, 'sp'), axis=0)  194 us
    psum x1, waiting for transfers between devices, together(): total = lax.psum(jnp.concatenate([a.ravel() for a in arrays]), axis)  113 us
    reduce_scatter x1, waiting for transfers between devices, on_device(): lax.psum_scatter(lax.dot_general(flat_s, flat_d, (((0,), (0,)), ((), ()))...  69.1 us
    unnamed x17, local copies, waits for them, and re-layouts  15.7 us
    dot_general x1, matrix products, on_device(): lax.dot_general(flat_s, flat_d, (((0,), (0,)), ((), ())), preferred_eleme...  15.4 us
    dot_general x1, matrix products, mechanism(): jnp.einsum('gts,insgc->intgc', w_low, normed, preferred_element_type=jnp....  14.9 us
    reduce_sum x1, other arithmetic, on_device(): grad_w_out = jnp.sum(lax.all_gather(partial_rows, 'sp'), axis=0)  13.1 us
    dot_general x1, matrix products, on_device(): lax.dot_general(d_out, lax.all_gather(w_out, 'dp', axis=0, tiled=True), (...  13.1 us
  transfers between devices with their start and end apart: 4, of which 4 were waited for; matrix products, arithmetic and copies ran while one was open for 20% of the time, Pallas kernels for 0%

profile of v1, /device:TPU:0, one launch (start us, length us, event | category | flops | bytes accessed | tf_op | source)
XLA Modules:
  0.0 589.0 jit_solution(8705468033260390832)
XLA Ops:
  7.2 0.7 all-gather.4.cloned.1.call-update
  7.9 3.2 convert_bitcast_fusion
  11.2 5.2 copy.67
  16.4 9.1 %copy.45 = f32[1,8,128,16,128]{2,4,1,3,0:T(8,128)} copy(f32[1,8,128,16,128]{4,3,0,2,1:T(8,128)} %bitcast.101) | data formatting | bytes 16777216 | tf_op jit(solution)/shard_map/reshape | solution.py:22
  25.5 3.2 convert_bitcast_fusion.1
  28.8 5.2 copy.65
  34.0 8.7 %copy.39 = f32[1,8,128,16,128]{2,4,1,3,0:T(8,128)} copy(f32[1,8,128,16,128]{4,3,0,2,1:T(8,128)} %bitcast.105) | data formatting | bytes 16777216 | tf_op jit(solution)/shard_map/reshape | solution.py:23
  42.8 6.0 %fusion.54 = f32[8,128,16]{1,0,2:T(8,128)S(1)} fusion(f32[1,8,128,16,128]{2,4,1,3,0:T(8,128)} %copy.39), kind=kLoop, calls=%fused_computation.83 | loop fusion | flops 18857984 | bytes 8454144 | tf_op jit(solution)/shard_map/reduce_sum | solution.py:27
  48.9 3.7 multiply_reduce_fusion.2
  52.7 6.5 %fusion.35 = bf16[8,128,16,128]{3,1,0,2:T(8,128)(2,1)} fusion(f32[8,128,16,128]{3,2,1,0:T(8,128)S(1)} %bitcast.106, f32[16,128]{1,0:T(8,128)S(1)} %copy-done.4, f32[16,128]{1,0:T(8,128)S(1)} %copy-done.3, f32[8,128,16]{1,0,2:T(8,128)S(1)} %add_rsqrt_fusion, f32[8,128,16]{1,0,2:T(8,128)S(1)} %broadcast_multiply_fusion.2), kind=kLoop, calls=%fused_computation.52 | loop fusion | flops 27262976 | bytes 12730368 | tf_op jit(solution)/shard_map/convert_element_type | solution.py:30
  59.1 2.7 all-gather.4.cloned.1.call-done
  61.8 13.1 %convert_bitcast_fusion.2 = f32[128,8,16,128]{3,1,2,0:T(8,128)S(1)} fusion(bf16[2048,2048]{1,0:T(8,128)(2,1)} %all-gather.4.cloned.1.call-done, bf16[1,1024,2048]{2,1,0:T(8,128)(2,1)} %param.10), kind=kOutput, calls=%fused_computation.51 | convolution fusion | flops 8594128896 | bytes 20971520 | tf_op jit(solution)/shard_map/dot_general | solution.py:64
  74.9 5.2 copy.64
  80.1 8.8 %copy.41 = f32[1,8,128,16,128]{2,4,1,3,0:T(8,128)} copy(f32[1,8,128,16,128]{4,3,2,1,0:T(8,128)} %bitcast.103) | data formatting | bytes 16777216 | tf_op jit(solution)/shard_map/reshape | solution.py:24
  88.9 14.9 %multiply_convert_fusion = (bf16[1,8,128,16,128]{2,4,1,3,0:T(8,128)(2,1)}, bf16[1,8,128,16,128]{2,4,1,3,0:T(8,128)(2,1)}, f32[128,16]{0,1:T(8,128)S(1)}) fusion(f32[128,16]{0,1:T(8,128)S(1)} %bitcast.114, f32[1,8,128,16,128]{2,4,1,3,0:T(8,128)} %copy.45, f32[1,8,128,16,128]{2,4,1,3,0:T(8,128)} %copy.41, bf16[8,128,16,128]{3,1,0,2:T(8,128)(2,1)} %fusion.35, ...), kind=kOutput, calls=%fused_computation.46 | convolution fusion | flops 593754112 | bytes 29917184 | tf_op jit(solution)/shard_map/gts,insgc->intgc/dot_general | solution.py:33
  103.8 6.8 %copy.58 = bf16[1,8,128,16,128]{4,3,2,1,0:T(8,128)(2,1)} copy(bf16[1,8,128,16,128]{2,4,1,3,0:T(8,128)(2,1)} %get-tuple-element.11) | data formatting | bytes 8388608 | tf_op jit(solution)/shard_map/convert_element_type | solution.py:35
  110.6 15.4 %fusion.37 = f32[2048,2048]{1,0:T(8,128)} fusion(bf16[128,8,16,128]{3,2,1,0:T(8,128)(2,1)} %bitcast.109, bf16[1,1024,2048]{2,1,0:T(8,128)(2,1)} %param.10), kind=kOutput, calls=%fused_computation.57 | convolution fusion | flops 8589934592 | bytes 25165824 | tf_op jit(solution)/shard_map/dot_general | solution.py:80
  126.0 10.2 %fusion.33 = bf16[8,128,16,128]{3,1,0,2:T(8,128)(2,1)S(1)} fusion(f32[8,128,16,128]{3,2,1,0:T(8,128)} %bitcast.104, f32[8,128,16,128]{3,2,1,0:T(8,128)} %bitcast.102), kind=kLoop, calls=%fused_computation.39 | loop fusion | flops 20971520 | bytes 20971520 | tf_op jit(solution)/shard_map/convert_element_type | solution.py:37
  136.2 1.3 fusion.45
  137.5 10.3 %fusion.34 = (f32[16,128]{1,0:T(8,128)S(1)}, f32[8,128,16]{1,0,2:T(8,128)S(1)}, f32[8,128,16]{1,0,2:T(8,128)S(1)}, f32[16,128]{1,0:T(8,128)S(1)}, f32[16,8,128,128]{3,2,1,0:T(8,128)}) fusion(f32[8,128,16]{1,0,2:T(8,128)S(1)} %add_rsqrt_fusion, f32[8,128,16]{1,0,2:T(8,128)S(1)} %broadcast_multiply_fusion.2, f32[1,8,128,16,128]{2,4,1,3,0:T(8,128)} %copy.39, ...), kind=kOutput, calls=%fused_computation.44 | convolution fusion | flops 572747776 | bytes 21798912 | tf_op jit(solution)/shard_map/gts,intgc->insgc/dot_general | solution.py:42
  147.8 1.0 pad_maximum_fusion
  148.9 69.1 %reduce-scatter.2.cloned.1.call-done = f32[256,2048]{1,0:T(8,128)} async-done(((f32[2048,2048]{1,0:T(8,128)}), f32[256,2048]{1,0:T(8,128)}) %reduce-scatter.2.cloned.1.call-update) | async-done | bytes 2097168 | tf_op jit(solution)/shard_map/reduce_scatter | solution.py:79
  218.1 6.9 %copy.47 = bf16[1,8,128,16,128]{4,3,2,1,0:T(8,128)(2,1)} copy(bf16[1,8,128,16,128]{2,4,1,3,0:T(8,128)(2,1)} %get-tuple-element.12) | data formatting | bytes 8388608 | tf_op jit(solution)/shard_map/convert_element_type | solution.py:38
  225.0 7.3 %reshape.497 = bf16[1,1024,2048]{2,1,0:T(8,128)(2,1)} reshape(bf16[1,8,128,16,128]{4,3,2,1,0:T(8,128)(2,1)} %copy.47) | data formatting | bytes 8388608 | tf_op jit(solution)/shard_map/reshape | solution.py:38
  232.3 12.2 %fusion.6 = bf16[1,8,128,16,128]{2,4,1,3,0:T(8,128)(2,1)} fusion(f32[1,8,128,16,128]{2,4,1,3,0:T(8,128)} %copy.39, f32[16,8,128,128]{3,2,1,0:T(8,128)} %get-tuple-element.17, f32[8,128,16]{1,0,2:T(8,128)S(1)} %get-tuple-element.18, f32[8,128,16]{1,0,2:T(8,128)S(1)} %get-tuple-element.19, f32[16,128]{1,0:T(8,128)S(1)} %copy-done.3, ...), kind=kLoop, calls=%fused_computation.12 | loop fusion | flops 58720256 | bytes 21241856 | tf_op jit(solution)/shard_map/convert_element_type | solution.py:51
  244.5 6.8 %copy.56 = bf16[1,8,128,16,128]{4,3,2,1,0:T(8,128)(2,1)} copy(bf16[1,8,128,16,128]{2,4,1,3,0:T(8,128)(2,1)} %fusion.6) | data formatting | bytes 8388608 | tf_op jit(solution)/shard_map/convert_element_type | solution.py:51
  251.3 7.3 %reshape.500 = bf16[1,1024,2048]{2,1,0:T(8,128)(2,1)} reshape(bf16[1,8,128,16,128]{4,3,2,1,0:T(8,128)(2,1)} %copy.56) | data formatting | bytes 8388608 | tf_op jit(solution)/shard_map/reshape | solution.py:51
  258.6 112.8 %all-reduce.2.cloned.1.call-done = f32[268288]{0:T(1024)} async-done(((f32[268288]{0:T(1024)}), f32[268288]{0:T(1024)}) %all-reduce.2.cloned.1.call-update) | async-done | bytes 1073168 | tf_op jit(solution)/shard_map/psum | solution.py:13
  371.4 2.3 slice.49
  373.7 1.3 slice_bitcast_fusion
  375.0 194.1 %all-gather.6.cloned.1.call-done = f32[4096,2048]{1,0:T(8,128)} async-done(((f32[256,2048]{1,0:T(8,128)}), f32[4096,2048]{1,0:T(8,128)}) %all-gather.6.cloned.1.call-update) | async-done | bytes 33554448 | tf_op jit(solution)/shard_map/all_gather | solution.py:87
  569.1 13.1 %reduce_sum.76 = f32[256,2048]{1,0:T(8,128)} reduce(f32[16,256,2048]{2,1,0:T(8,128)} %bitcast.107, f32[]{:T(128)} %constant.9.clone.1), dimensions={0}, to_apply=%region_5.6 | reduce | flops 7864320 | bytes 35651588 | tf_op jit(solution)/shard_map/reduce_sum | solution.py:87
  (25 shorter events, 0.4 us)
Async XLA Ops:
  7.2 54.7 %all-gather.4.cloned.1.call-start = ((), (), s32[]{:S(2)}) async-start(), calls=%async_computation.1 | async-start | bytes 9437184 | tf_op jit(solution)/shard_map/all_gather | solution.py:66
  7.9 210.2 %reduce-scatter.2.cloned.1.call-start = ((), (), s32[]{:S(2)}) async-start(), calls=%async_computation.2 | async-start | bytes 18874368 | tf_op jit(solution)/shard_map/reduce_scatter | solution.py:79
  42.7 6.2 %copy-start = (f32[1,8,128,16,128]{2,4,1,3,0:T(8,128)S(1)}, f32[1,8,128,16,128]{2,4,1,3,0:T(8,128)}, u32[]{:S(2)}) copy-start(f32[1,8,128,16,128]{2,4,1,3,0:T(8,128)} %copy.39) | copy-start | bytes 25165828
  42.7 9.9 %copy-start.1 = (f32[128,8,16,128]{3,2,1,0:T(8,128)S(1)}, f32[128,8,16,128]{3,2,1,0:T(8,128)}, u32[]{:S(2)}) copy-start(f32[128,8,16,128]{3,2,1,0:T(8,128)} %copy.65) | copy-start | bytes 25165828
  42.7 9.9 %copy-start.3 = (f32[16,128]{1,0:T(8,128)S(1)}, f32[16,128]{1,0:T(8,128)}, u32[]{:S(2)}) copy-start(f32[16,128]{1,0:T(8,128)} %param.13) | copy-start | bytes 24580
  42.7 9.9 %copy-start.4 = (f32[16,128]{1,0:T(8,128)S(1)}, f32[16,128]{1,0:T(8,128)}, u32[]{:S(2)}) copy-start(f32[16,128]{1,0:T(8,128)} %param.14) | copy-start | bytes 24580
  80.1 8.8 %copy-start.5 = (bf16[16,128,128]{2,1,0:T(8,128)(2,1)S(1)}, bf16[16,128,128]{2,1,0:T(8,128)(2,1)}, u32[]{:S(2)}) copy-start(bf16[16,128,128]{2,1,0:T(8,128)(2,1)} %param.11) | copy-start | bytes 1572868
  80.1 8.8 %copy-start.6 = (f32[16,128]{1,0:T(8,128)S(1)}, f32[16,128]{1,0:T(8,128)}, u32[]{:S(2)}) copy-start(f32[16,128]{1,0:T(8,128)} %param.12) | copy-start | bytes 24580
  126.0 245.4 %all-reduce.2.cloned.1.call-start = ((), (), s32[]{:S(2)}) async-start(), calls=%async_computation.3 | async-start | bytes 2146304 | tf_op jit(solution)/shard_map/psum | solution.py:13
  126.0 10.2 %copy-start.2 = (bf16[8,128,16,128]{3,1,0,2:T(8,128)(2,1)S(1)}, bf16[8,128,16,128]{3,1,0,2:T(8,128)(2,1)}, u32[]{:S(2)}) copy-start(bf16[8,128,16,128]{3,1,0,2:T(8,128)(2,1)} %fusion.35) | copy-start | bytes 12582916
  148.9 420.3 %all-gather.6.cloned.1.call-start = ((), (), s32[]{:S(2)}) async-start(), calls=%async_computation.4 | async-start | bytes 35651584 | tf_op jit(solution)/shard_map/all_gather | solution.py:87
Sparse Core Ops, SparseCore 0:
  9.7 52.0 all-gather.3
  126.1 91.9 reduce-scatter.1
  223.4 147.9 all-reduce.1
  373.4 195.6 all-gather.5
